TPU v7x, 128 devices: a whole 4x4x4 slice. The times are simulated.
128 devices in a mesh: ep: 64 (over z, y, x), tp: 2 (over core).
Axes of the slice: x: 4, y: 4, z: 4, core: 2. Of those that a mesh axis runs over, the one named last changes fastest.
Arguments:
- tokens: bfloat16 [1024, 2048], P('ep'), may hold values from -6 to 6
- norm_gain: float32 [2048], replicated, may hold values from 0.1 to 1.9
- query_weight: bfloat16 [2048, 1024], P('ep', 'tp'), may hold values from -0.125 to 0.125
- key_weight: bfloat16 [2048, 1024], P('ep', 'tp'), may hold values from -0.125 to 0.125
- value_weight: bfloat16 [2048, 1024], P('ep', 'tp'), may hold values from -0.125 to 0.125
- outgate_weight: bfloat16 [2048, 1024], P('ep', 'tp'), may hold values from -0.125 to 0.125
- input_weight: bfloat16 [2048, 8], P('ep', 'tp'), may hold values from -0.125 to 0.125
- forget_weight: bfloat16 [2048, 8], P('ep', 'tp'), may hold values from -0.125 to 0.125
- forget_bias: float32 [8], P('tp'), may hold values from -1 to 5
- memory: float32 [1024, 8, 128, 128], P('ep', 'tp'), may hold values from -2.4 to 2.4
- stabilizer: float32 [1024, 8], P('ep', 'tp'), may hold values from -3 to 3
- head_gain: float32 [1024], P('tp'), may hold values from 0.1 to 1.9
- mix_weight: bfloat16 [1024, 2048], P('tp', 'ep'), may hold values from -0.1875 to 0.1875
- second_gain: float32 [2048], replicated, may hold values from 0.1 to 1.9
- route_experts: int32 [1024, 4], P('ep'), may hold values from 0 to 63, all different within a row; in each aligned block of 16 rows (0 to 15, 16 to 31, ...) at most 2 rows name the same one
- route_weight: float32 [1024, 4], P('ep'), may hold values from 0.1 to 1
- expert_gate: bfloat16 [64, 2048, 2048], P('ep', None, 'tp'), may hold values from -0.5 to 0.5
- expert_up: bfloat16 [64, 2048, 2048], P('ep', None, 'tp'), may hold values from -0.5 to 0.5
- expert_down: bfloat16 [64, 2048, 2048], P('ep', 'tp'), may hold values from -0.03125 to 0.03125
- dense_gate: bfloat16 [4096, 2048], P(('ep', 'tp')), may hold values from -0.125 to 0.125
- dense_up: bfloat16 [4096, 2048], P(('ep', 'tp')), may hold values from -0.125 to 0.125
- dense_down: bfloat16 [4096, 2048], P(('ep', 'tp')), may hold values from -0.09375 to 0.09375
- branch_scale: float32 [2048], replicated, may hold values from 0.3 to 1.5
Outputs:
- mixed: bfloat16 [1024, 2048], P('ep', 'tp')
- memory_new: float32 [1024, 8, 128, 128], P('ep', 'tp')
- stabilizer_new: float32 [1024, 8], P('ep', 'tp')
Inputs may be any that keep to these rules, and one draw needn't show every extreme that they name: `route_experts`: each row names 4 different experts. Within each aligned block of 16 rows no expert is named by more than 2 rows, and in every draw some expert is named by exactly 2 rows of some block.
All inputs are finite; a program needn't handle non-finite values.
Results may differ from a plain program's by a relative error of at most 0.03.
Values may be sent and summed in bfloat16 or wider, within the bound.
A program may use at most 128 MiB of HBM per device.

v0:
```python
import jax
import jax.numpy as jnp
from jax import lax
from jax.sharding import PartitionSpec as P

norm_eps = 1e-05
clamp_limit = 7.0
sigmoid_slope = 1.702


def in_one_piece(arrays, axis, dim, along):
    widths = [a.shape[along] for a in arrays]
    both = jnp.concatenate(arrays, axis=along)
    whole = lax.all_gather(both, axis, axis=dim, tiled=True)
    return tuple(jnp.split(whole, [sum(widths[:k]) for k in range(1, len(widths))], axis=along))


def sent_to_all(shard, axis):
    devices = lax.axis_size(axis)
    return lax.all_to_all(
        jnp.broadcast_to(shard[None], (devices, *shard.shape)), axis, 0, 0, tiled=True
    )


def taken_together(shard, axis):
    return sent_to_all(shard, axis).astype(jnp.float32).sum(axis=0)


def cut_along(shard, dim, devices):
    lengths = shard.shape
    pieces = shard.reshape(*lengths[:dim], devices, lengths[dim] // devices, *lengths[dim + 1 :])
    return jnp.moveaxis(pieces, dim, 0)


def sent_and_summed(shard, axis, dim):
    devices = lax.axis_size(axis)
    pieces = lax.all_to_all(cut_along(shard, dim, devices), axis, 0, 0, tiled=True)
    return jnp.sum(pieces.astype(jnp.float32), axis=0)


def rms_scale(values, gain):
    mean_square = jnp.mean(values * values, axis=-1, keepdims=True)
    return values * lax.rsqrt(mean_square + norm_eps) * gain


def round_half(values):
    return lax.optimization_barrier(values.astype(jnp.bfloat16)).astype(jnp.float32)


def clamped_unit(gate_pre, up_pre):
    gate_clamped = jnp.minimum(gate_pre, clamp_limit)
    up_clamped = jnp.clip(up_pre, -clamp_limit, clamp_limit)
    return (
        (up_clamped + 1.0) * gate_clamped * jax.nn.sigmoid(sigmoid_slope * gate_clamped)
    ).astype(jnp.bfloat16)


def memory_step(projected, forget_bias, memory, stabilizer, head_gain):
    query_rows, key_rows, value_rows, outgate_rows, input_pre, forget_pre = projected
    sequences, head_count = stabilizer.shape
    head_size = memory.shape[-1]
    log_forget = jax.nn.log_sigmoid(forget_pre + forget_bias)
    stab_new = jnp.maximum(log_forget + stabilizer, input_pre)
    carried = jnp.exp(log_forget + stabilizer - stab_new)
    written = jnp.exp(input_pre - stab_new)
    query_heads = query_rows.astype(jnp.float32).reshape(sequences, head_count, head_size)
    key_heads = key_rows.astype(jnp.float32).reshape(
        sequences, head_count, head_size
    ) * head_size ** (-0.5)
    value_heads = value_rows.astype(jnp.float32).reshape(sequences, head_count, head_size)
    memory_new = (
        carried[:, :, None, None] * memory
        + written[:, :, None, None] * value_heads[:, :, :, None] * key_heads[:, :, None, :]
    )
    readout = jnp.einsum("bhvk,bhk->bhv", memory_new, query_heads)
    out_gate = jax.nn.sigmoid(
        outgate_rows.astype(jnp.float32).reshape(sequences, head_count, head_size)
    )
    gated = (rms_scale(readout, head_gain.reshape(head_count, head_size)) * out_gate).astype(
        jnp.bfloat16
    )
    return (gated.reshape(sequences, head_count * head_size), memory_new, stab_new)


def expert_apply(rows, gate_weight, up_weight, down_weight):
    gate_pre = jnp.dot(rows, gate_weight, preferred_element_type=jnp.float32)
    up_pre = jnp.dot(rows, up_weight, preferred_element_type=jnp.float32)
    activity = clamped_unit(gate_pre, up_pre)
    return jnp.dot(activity, down_weight, preferred_element_type=jnp.float32).astype(jnp.bfloat16)


def slot_table(hit_mask, capacity):
    ranks = jnp.cumsum(hit_mask, axis=1) - 1.0
    slots = jnp.arange(capacity).astype(jnp.float32)
    return hit_mask[:, None, :] * (ranks[:, None, :] == slots[None, :, None]).astype(jnp.float32)


def body(
    tokens,
    norm_gain,
    query_weight,
    key_weight,
    value_weight,
    outgate_weight,
    input_weight,
    forget_weight,
    forget_bias,
    memory,
    stabilizer,
    head_gain,
    mix_weight,
    second_gain,
    route_experts,
    route_weight,
    expert_gate,
    expert_up,
    expert_down,
    dense_gate,
    dense_up,
    dense_down,
    branch_scale,
):
    sequences, model_width = tokens.shape
    ep_count = lax.axis_size("ep")
    tp_count = lax.axis_size("tp")
    part_width = model_width // tp_count
    top_count = route_experts.shape[1]
    expert_count = expert_gate.shape[0] * ep_count
    capacity = max(2, 2 * sequences * top_count // expert_count)
    inputs_float = tokens.astype(jnp.float32)
    normed = rms_scale(inputs_float, norm_gain).astype(jnp.bfloat16)
    pieces = in_one_piece(
        (query_weight, key_weight, value_weight, outgate_weight, input_weight, forget_weight),
        "ep",
        0,
        1,
    )
    sums = tuple((jnp.dot(normed, piece, preferred_element_type=jnp.float32) for piece in pieces))
    projected = (
        sums[0].astype(jnp.bfloat16),
        sums[1].astype(jnp.bfloat16),
        sums[2].astype(jnp.bfloat16),
        sums[3].astype(jnp.bfloat16),
        sums[4],
        sums[5],
    )
    gated, memory_new, stab_new = memory_step(projected, forget_bias, memory, stabilizer, head_gain)
    partial_value = jnp.dot(
        gated,
        lax.all_gather(mix_weight, "ep", axis=1, tiled=True),
        preferred_element_type=jnp.float32,
    )
    attended = taken_together(round_half(partial_value).astype(jnp.bfloat16), "tp").astype(
        jnp.float32
    )
    residual = (inputs_float + attended).astype(jnp.bfloat16)
    residual_float = residual.astype(jnp.float32)
    normed_second = rms_scale(residual_float, second_gain).astype(jnp.bfloat16)
    own_residual = lax.dynamic_slice_in_dim(
        residual_float, lax.axis_index("tp") * part_width, part_width, 1
    )
    own_scale = lax.dynamic_slice_in_dim(
        branch_scale, lax.axis_index("tp") * part_width, part_width, 0
    )
    matched = route_experts[:, :, None] == jnp.arange(expert_count)[None, None, :]
    hit_mask = jnp.any(matched, axis=1).astype(jnp.float32).T
    weights = jnp.sum(jnp.where(matched, route_weight[:, :, None], 0.0), axis=1).T
    select = slot_table(hit_mask, capacity)
    outgoing = jnp.einsum(
        "ecs,sd->ecd",
        select.astype(jnp.bfloat16),
        normed_second,
        preferred_element_type=jnp.float32,
    ).astype(jnp.bfloat16)
    received = lax.all_to_all(outgoing, "ep", split_axis=0, concat_axis=0, tiled=True)
    count = received.shape[1]
    partial_out = expert_apply(
        received.reshape(-1, model_width), expert_gate[0], expert_up[0], expert_down[0]
    )
    halves = sent_and_summed(partial_out.astype(jnp.float32).astype(jnp.bfloat16), "tp", 1)
    returned = lax.all_to_all(
        halves.reshape(ep_count, count, part_width).astype(jnp.bfloat16),
        "ep",
        split_axis=0,
        concat_axis=0,
        tiled=True,
    ).astype(jnp.float32)
    routed = jnp.einsum("ecs,ecd->sd", select * weights[:, None, :], returned)
    gate_piece, up_piece, down_piece = in_one_piece((dense_gate, dense_up, dense_down), "ep", 0, 1)
    gate_rows = jnp.einsum(
        "td,fd->tf", normed_second, gate_piece, preferred_element_type=jnp.float32
    )
    lift_rows = jnp.einsum("td,fd->tf", normed_second, up_piece, preferred_element_type=jnp.float32)
    activity = (jax.nn.silu(gate_rows) * lift_rows).astype(jnp.bfloat16)
    total = jnp.dot(activity, down_piece, preferred_element_type=jnp.float32)
    halves = sent_and_summed(total.astype(jnp.bfloat16), "tp", 1)
    branch = halves * own_scale
    mixed = own_residual + routed + branch
    return (mixed.astype(jnp.bfloat16), memory_new, stab_new)


def solution(mesh):
    in_specs = (
        P("ep", None),
        P(),
        P("ep", "tp"),
        P("ep", "tp"),
        P("ep", "tp"),
        P("ep", "tp"),
        P("ep", "tp"),
        P("ep", "tp"),
        P("tp"),
        P("ep", "tp", None, None),
        P("ep", "tp"),
        P("tp"),
        P("tp", "ep"),
        P(),
        P("ep", None),
        P("ep", None),
        P("ep", None, "tp"),
        P("ep", None, "tp"),
        P("ep", "tp", None),
        P(("ep", "tp"), None),
        P(("ep", "tp"), None),
        P(("ep", "tp"), None),
        P(),
    )
    out_specs = (P("ep", "tp"), P("ep", "tp", None, None), P("ep", "tp"))
    return jax.shard_map(body, mesh=mesh, in_specs=in_specs, out_specs=out_specs, check_vma=False)
```

profile of v0, /device:TPU:0, one launch (start us, length us, event | category | flops | bytes accessed | tf_op | source)
XLA Modules:
  0.0 342.2 jit_solution(8388457338373234706)
XLA Ops:
  7.2 0.8 copy.56
  8.0 0.8 copy.57
  8.8 1.5 concatenate.6
  10.4 0.7 all-gather.6.cloned.1.call-update
  11.2 1.8 pad_maximum_fusion
  13.0 0.8 fusion.119
  14.1 1.0 fusion.107
  15.1 78.9 %all-gather.4.cloned.1.call-done = bf16[2048,2056]{1,0:T(8,128)(2,1)} async-done(((bf16[32,2056]{1,0:T(8,128)(2,1)}), bf16[2048,2056]{1,0:T(8,128)(2,1)}) %all-gather.4.cloned.1.call-update) | async-done | bytes 8421392 | tf_op jit(solution)/shard_map/all_gather | solution.py:14
  94.0 1.3 fusion.94
  95.3 1.8 subtract_exponential_fusion.1
  97.2 2.1 fusion.58
  99.4 2.0 fusion.67
  101.4 2.0 fusion.70
  103.4 2.0 fusion.88
  105.6 3.1 multiply_add_fusion
  108.7 2.0 copy-done
  110.7 1.2 fusion.149
  112.1 49.8 %all-gather.6.cloned.1.call-done = bf16[512,2048]{0,1:T(8,128)(2,1)} async-done(((bf16[512,32]{0,1:T(8,128)(2,1)}), bf16[512,2048]{0,1:T(8,128)(2,1)}) %all-gather.6.cloned.1.call-update) | async-done | bytes 2097168 | tf_op jit(solution)/shard_map/all_gather | solution.py:150
  161.8 2.2 convolution_convert_fusion.1
  164.1 3.8 %all_to_all.25 = bf16[2,16,2048]{2,1,0:T(8,128)(2,1)S(1)} all-to-all(bf16[2,16,2048]{2,1,0:T(8,128)(2,1)S(1)} %broadcast_in_dim.10), channel_id=1, replica_groups=mesh['ep'=64,'tp'=2] {'tp'}, dimensions={0} | all-to-all | bytes 262144 | tf_op jit(solution)/shard_map/all_to_all | solution.py:20
  169.2 22.5 %all_to_all.26 = bf16[64,2,2048]{2,1,0:T(2,128)(2,1)S(1)} all-to-all(bf16[64,2,2048]{2,1,0:T(2,128)(2,1)S(1)} %copy.62), channel_id=1, replica_groups=mesh['ep'=64,'tp'=2] {'ep'}, dimensions={0} | all-to-all | bytes 1048576 | tf_op jit(solution)/shard_map/all_to_all | solution.py:175
  191.9 2.9 fusion.37
  194.8 5.5 %fusion.12 = bf16[128,2048]{1,0:T(8,128)(2,1)S(1)} fusion(bf16[1,1024,2048]{2,1,0:T(8,128)(2,1)} %param.41, f32[128,1024]{1,0:T(8,128)S(1)} %fusion.37, bf16[128,2048]{1,0:T(8,128)(2,1)S(1)} %reshape.97, bf16[1,2048,1024]{2,1,0:T(8,128)(2,1)} %param.40), kind=kOutput, calls=%fused_computation.13 | convolution fusion | flops 1075183616 | bytes 9961472 | tf_op jit(solution)/shard_map/dot_general | solution.py:89
  200.4 4.2 %all_to_all.27 = bf16[2,128,1024]{2,1,0:T(8,128)(2,1)S(1)} all-to-all(bf16[2,128,1024]{2,1,0:T(8,128)(2,1)S(1)} %bitcast.67), channel_id=1, replica_groups=mesh['ep'=64,'tp'=2] {'tp'}, dimensions={0} | all-to-all | bytes 1048576 | tf_op jit(solution)/shard_map/all_to_all | solution.py:37
  204.6 0.8 convert_element_type.114
  205.4 91.2 %all-gather.8.cloned.1.call-done = bf16[2048,6144]{1,0:T(8,128)(2,1)} async-done(((bf16[32,6144]{1,0:T(8,128)(2,1)}), bf16[2048,6144]{1,0:T(8,128)(2,1)}) %all-gather.8.cloned.1.call-update) | async-done | bytes 25165840 | tf_op jit(solution)/shard_map/all_gather | solution.py:14
  296.6 5.6 %fusion.4 = f32[16,2048]{1,0:T(8,128)S(1)} fusion(bf16[16,2048]{1,0:T(8,128)(2,1)S(1)} %multiply_convert_fusion, bf16[2048,6144]{1,0:T(8,128)(2,1)} %all-gather.8.cloned.1.call-done), kind=kOutput, calls=%fused_computation.4 | convolution fusion | flops 134217728 | bytes 8585216 | tf_op jit(solution)/shard_map/td,fd->tf/dot_general | solution.py:190
  302.3 9.2 %fusion.21 = bf16[16,2048]{1,0:T(8,128)(2,1)S(1)} fusion(bf16[2048,6144]{1,0:T(8,128)(2,1)} %all-gather.8.cloned.1.call-done, bf16[16,2048]{1,0:T(8,128)(2,1)S(1)} %multiply_convert_fusion, f32[16,2048]{1,0:T(8,128)S(1)} %fusion.4), kind=kOutput, calls=%fused_computation.17 | convolution fusion | flops 268664832 | bytes 17039360 | tf_op jit(solution)/shard_map/dot_general | solution.py:195
  311.5 3.8 %all_to_all.28 = bf16[2,16,1024]{2,1,0:T(8,128)(2,1)S(1)} all-to-all(bf16[2,16,1024]{2,1,0:T(8,128)(2,1)S(1)} %bitcast.71), channel_id=1, replica_groups=mesh['ep'=64,'tp'=2] {'tp'}, dimensions={0} | all-to-all | bytes 131072 | tf_op jit(solution)/shard_map/all_to_all | solution.py:37
  315.2 8.6 %all-to-all-start.3 = ((bf16[64,2,1024]{2,1,0:T(2,128)(2,1)}), bf16[64,2,1024]{2,1,0:T(2,128)(2,1)S(1)}, u32[]{:S(2)}, u32[]{:S(2)}) async-start(bf16[64,2,1024]{2,1,0:T(2,128)(2,1)} %convert_element_type.114), calls=%async_computation.3 | async-start | bytes 524288 | tf_op jit(solution)/shard_map/all_to_all | solution.py:181
  324.0 10.8 %all-to-all-done.3 = bf16[64,2,1024]{2,1,0:T(2,128)(2,1)S(1)} async-done(((bf16[64,2,1024]{2,1,0:T(2,128)(2,1)}), bf16[64,2,1024]{2,1,0:T(2,128)(2,1)S(1)}, u32[]{:S(2)}, u32[]{:S(2)}) %all-to-all-start.3) | async-done | bytes 262176 | tf_op jit(solution)/shard_map/all_to_all | solution.py:181
  334.8 0.9 fusion.54
  (54 shorter events, 2.7 us)
Async XLA Ops:
  7.2 92.2 %copy-start.1 = (bf16[16,2048]{1,0:T(8,128)(2,1)S(1)}, bf16[16,2048]{1,0:T(8,128)(2,1)}, u32[]{:S(2)}) copy-start(bf16[16,2048]{1,0:T(8,128)(2,1)} %param.23) | copy-start | bytes 196612
  7.2 92.2 %copy-start.8 = (f32[2048]{0:T(1024)S(1)}, f32[2048]{0:T(1024)}, u32[]{:S(2)}) copy-start(f32[2048]{0:T(1024)} %param.24) | copy-start | bytes 24580
  7.2 86.8 %all-gather.4.cloned.1.call-start = ((), (), s32[]{:S(2)}) async-start(), calls=%async_computation.5 | async-start | bytes 9052160 | tf_op jit(solution)/shard_map/all_gather | solution.py:14
  10.4 151.5 %all-gather.6.cloned.1.call-start = ((), (), s32[]{:S(2)}) async-start(), calls=%async_computation.6 | async-start | bytes 2129920 | tf_op jit(solution)/shard_map/all_gather | solution.py:150
  11.1 285.5 %all-gather.8.cloned.1.call-start = ((), (), s32[]{:S(2)}) async-start(), calls=%async_computation.7 | async-start | bytes 25559040 | tf_op jit(solution)/shard_map/all_gather | solution.py:14
  97.1 8.4 %copy-start.5 = (f32[16,4]{0,1:T(4,128)}, f32[16,4]{0,1:T(4,128)S(1)}, u32[]{:S(2)}) copy-start(f32[16,4]{0,1:T(4,128)S(1)} %get-tuple-element.6) | copy-start | bytes 772
  108.7 2.0 copy-start
  110.7 1.3 copy-start.4
  110.7 57.5 %copy-start.2 = (f32[2048]{0:T(1024)S(1)}, f32[2048]{0:T(1024)}, u32[]{:S(2)}) copy-start(f32[2048]{0:T(1024)} %param.36) | copy-start | bytes 24580
  302.2 21.6 %copy-start.6 = (f32[2048]{0:T(1024)S(1)}, f32[2048]{0:T(1024)}, u32[]{:S(2)}) copy-start(f32[2048]{0:T(1024)} %param.45) | copy-start | bytes 24580
  302.2 21.7 %copy-start.3 = (s32[16,4]{0,1:T(4,128)S(1)}, s32[16,4]{0,1:T(4,128)}, u32[]{:S(2)}) copy-start(s32[16,4]{0,1:T(4,128)} %param.37) | copy-start | bytes 772
  302.2 21.7 %copy-start.7 = (f32[16,4]{0,1:T(4,128)S(1)}, f32[16,4]{0,1:T(4,128)}, u32[]{:S(2)}) copy-start(f32[16,4]{0,1:T(4,128)} %param.38) | copy-start | bytes 772
  315.2 19.5 %all-to-all-start.3 = ((bf16[64,2,1024]{2,1,0:T(2,128)(2,1)}), bf16[64,2,1024]{2,1,0:T(2,128)(2,1)S(1)}, u32[]{:S(2)}, u32[]{:S(2)}) async-start(bf16[64,2,1024]{2,1,0:T(2,128)(2,1)} %convert_element_type.114), calls=%async_computation.3 | async-start | bytes 524288 | tf_op jit(solution)/shard_map/all_to_all | solution.py:181
Sparse Core Ops, SparseCore 0:
  11.3 82.5 all-gather.3
  96.8 64.9 all-gather.5
  164.6 131.9 all-gather.7
where the time goes:
time: 343 us; the launch traced here: 342 us
  waiting for transfers between devices  231 us (67%)
  matrix products  39.2 us (11%)
  blocking collectives  34.3 us (10%)
  between operations  14 us (4%)
  starting transfers between devices  8.72 us (3%)
  other arithmetic  7.55 us (2%)
  local copies, waits for them, and re-layouts  7.16 us (2%)
    all_gather x2, waiting for transfers between devices, in_one_piece(): whole = lax.all_gather(both, axis, axis=dim, tiled=True)  170 us
    all_gather x1, waiting for transfers between devices, body(): lax.all_gather(mix_weight, 'ep', axis=1, tiled=True)  49.8 us
    all_to_all x1, blocking collectives, body(): lax.all_to_all(outgoing, 'ep', split_axis=0, concat_axis=0, tiled=True)  22.5 us
    dot_general x6, matrix products, body(): jnp.dot(normed, piece, preferred_element_type=jnp.float32)  11.2 us
    all_to_all x1, waiting for transfers between devices, body(): lax.all_to_all(halves.reshape(ep_count, count, part_width).astype(jnp.bfl...  10.8 us
    dot_general x1, matrix products, body(): total = jnp.dot(activity, down_piece, preferred_element_type=jnp.float32)  9.18 us
    all_to_all x1, starting transfers between devices, body(): lax.all_to_all(halves.reshape(ep_count, count, part_width).astype(jnp.bfl...  8.6 us
    all_to_all x2, blocking collectives, sent_and_summed(): lax.all_to_all(cut_along(shard, dim, devices), axis, 0, 0, tiled=True)  7.95 us
  transfers between devices with their start and end apart: 4, of which 4 were waited for; matrix products, arithmetic and copies ran while one was open for 10% of the time, Pallas kernels for 0%

commit v1 on v0

--- a/solution.py
+++ b/solution.py
@@ -6,6 +6,14 @@
 norm_eps = 1e-05
 clamp_limit = 7.0
 sigmoid_slope = 1.702
+
+
+def records_find(mine, named_axis):
+    dev_n = jax.lax.axis_size(named_axis)
+    store = tuple((dev_n if idx == 1 else 1 for idx in range(mine.ndim)))
+    return jax.lax.all_to_all(
+        jnp.tile(mine, store), named_axis, split_axis=1, concat_axis=1, tiled=True
+    )
 
 
 def in_one_piece(arrays, axis, dim, along):
@@ -146,9 +154,7 @@
     )
     gated, memory_new, stab_new = memory_step(projected, forget_bias, memory, stabilizer, head_gain)
     partial_value = jnp.dot(
-        gated,
-        lax.all_gather(mix_weight, "ep", axis=1, tiled=True),
-        preferred_element_type=jnp.float32,
+        gated, records_find(mix_weight, "ep"), preferred_element_type=jnp.float32
     )
     attended = taken_together(round_half(partial_value).astype(jnp.bfloat16), "tp").astype(
         jnp.float32

time: 343 us -> 295 us (0.86)
  waiting for transfers between devices: 231 us -> 169 us
  starting transfers between devices: 8.72 us -> 20.2 us
  blocking collectives: 34.3 us -> 38.1 us
    all_gather x1 -> x0, waiting for transfers between devices: 49.8 us -> none  [body(): lax.all_gather(mix_weight, 'ep', axis=1, tiled=True)]
    all_gather x2, waiting for transfers between devices: 170 us -> 158 us  [in_one_piece(): whole = lax.all_gather(both, axis, axis=dim, tiled=True)]
    all_to_all x0 -> x1, starting transfers between devices: none -> 11.5 us  [records_find(): jax.lax.all_to_all(jnp.tile(mine, store), named_axis, split_axis=1, conca...]
    all_to_all x1, blocking collectives: 22.5 us -> 26.4 us  [body(): lax.all_to_all(outgoing, 'ep', split_axis=0, concat_axis=0, tiled=True)]
  transfers between devices with their start and end apart: 4 -> 4, of which waited for: 4 -> 3; matrix products, arithmetic and copies ran while one was open for 10% -> 11% of each run, Pallas kernels for 0% -> 0%
where the time goes in v1:
time: 295 us; the launch traced here: 294 us
  waiting for transfers between devices  169 us (57%)
  blocking collectives  38.1 us (13%)
  matrix products  37 us (13%)
  starting transfers between devices  20.2 us (7%)
  between operations  14.4 us (5%)
  local copies, waits for them, and re-layouts  9.45 us (3%)
  other arithmetic  6.15 us (2%)
    all_gather x2, waiting for transfers between devices, in_one_piece(): whole = lax.all_gather(both, axis, axis=dim, tiled=True)  158 us
    all_to_all x1, blocking collectives, body(): lax.all_to_all(outgoing, 'ep', split_axis=0, concat_axis=0, tiled=True)  26.4 us
    all_to_all x1, starting transfers between devices, records_find(): jax.lax.all_to_all(jnp.tile(mine, store), named_axis, split_axis=1, conca...  11.5 us
    dot_general x6, matrix products, body(): jnp.dot(normed, piece, preferred_element_type=jnp.float32)  11 us
    all_to_all x1, waiting for transfers between devices, body(): lax.all_to_all(halves.reshape(ep_count, count, part_width).astype(jnp.bfl...  10.8 us
    dot_general x1, matrix products, body(): total = jnp.dot(activity, down_piece, preferred_element_type=jnp.float32)  9.19 us
    all_to_all x1, starting transfers between devices, body(): lax.all_to_all(halves.reshape(ep_count, count, part_width).astype(jnp.bfl...  8.6 us
    all_to_all x2, blocking collectives, sent_and_summed(): lax.all_to_all(cut_along(shard, dim, devices), axis, 0, 0, tiled=True)  7.95 us
  transfers between devices with their start and end apart: 4, of which 3 were waited for; matrix products, arithmetic and copies ran while one was open for 11% of the time, Pallas kernels for 0%

profile of v1, /device:TPU:0, one launch (start us, length us, event | category | flops | bytes accessed | tf_op | source)
XLA Modules:
  0.0 294.3 jit_solution(6559463762706027675)
XLA Ops:
  7.2 0.8 copy.57
  8.0 0.8 copy.58
  8.8 1.5 concatenate.6
  10.4 1.8 pad_maximum_fusion
  12.3 2.3 tile.2
  14.6 11.5 %all-to-all-start = ((bf16[512,64,32]{0,2,1:T(8,128)(2,1)}), bf16[512,64,32]{0,2,1:T(8,128)(2,1)S(1)}, u32[]{:S(2)}, u32[]{:S(2)}) async-start(bf16[512,64,32]{0,2,1:T(8,128)(2,1)} %tile.2), calls=%async_computation | async-start | bytes 4194304 | tf_op jit(solution)/shard_map/all_to_all | solution.py:14
  26.7 84.1 %all-gather.3.cloned.1.call-done = bf16[2048,2056]{1,0:T(8,128)(2,1)} async-done(((bf16[32,2056]{1,0:T(8,128)(2,1)}), bf16[2048,2056]{1,0:T(8,128)(2,1)}) %all-gather.3.cloned.1.call-update) | async-done | bytes 8421392 | tf_op jit(solution)/shard_map/all_gather | solution.py:22
  110.8 1.3 fusion.94
  112.1 1.7 subtract_exponential_fusion.1
  113.9 2.0 fusion.58
  116.0 2.0 fusion.67
  118.1 2.0 fusion.70
  120.1 2.0 fusion.88
  122.3 3.2 %multiply_add_fusion = f32[16,4,128,128]{3,2,1,0:T(8,128)S(1)} fusion(f32[16,4,128,128]{3,2,1,0:T(8,128)} %param.32, f32[16,4,128]{2,1,0:T(4,128)S(1)} %mul.168, f32[16,4,128]{2,1,0:T(4,128)S(1)} %broadcast_multiply_fusion, f32[16,4]{1,0:T(8,128)S(1)} %copy.59), kind=kLoop, calls=%fused_computation.12 | loop fusion | flops 3145728 | bytes 8454400 | tf_op jit(solution)/shard_map/add | solution.py:80
  125.5 2.0 copy-done
  127.5 1.2 fusion.149
  128.9 0.6 convolution_convert_fusion.1
  129.6 3.8 %all_to_all.34 = bf16[2,16,2048]{2,1,0:T(8,128)(2,1)S(1)} all-to-all(bf16[2,16,2048]{2,1,0:T(8,128)(2,1)S(1)} %broadcast_in_dim.10), channel_id=1, replica_groups=mesh['ep'=64,'tp'=2] {'tp'}, dimensions={0} | all-to-all | bytes 262144 | tf_op jit(solution)/shard_map/all_to_all | solution.py:28
  133.7 0.4 convolution_convert_fusion
  134.1 0.5 copy.63
  134.6 26.4 %all_to_all.35 = bf16[64,2,2048]{2,1,0:T(2,128)(2,1)S(1)} all-to-all(bf16[64,2,2048]{2,1,0:T(2,128)(2,1)S(1)} %copy.63), channel_id=1, replica_groups=mesh['ep'=64,'tp'=2] {'ep'}, dimensions={0} | all-to-all | bytes 1048576 | tf_op jit(solution)/shard_map/all_to_all | solution.py:181
  161.2 3.0 %fusion.37 = f32[128,1024]{1,0:T(8,128)S(1)} fusion(bf16[128,2048]{1,0:T(8,128)(2,1)S(1)} %reshape.104, bf16[1,2048,1024]{2,1,0:T(8,128)(2,1)} %param.39), kind=kOutput, calls=%fused_computation.28 | convolution fusion | flops 537001984 | bytes 5242880 | tf_op jit(solution)/shard_map/dot_general | solution.py:94
  164.2 5.0 %fusion.12 = bf16[128,2048]{1,0:T(8,128)(2,1)S(1)} fusion(bf16[1,1024,2048]{2,1,0:T(8,128)(2,1)} %param.41, f32[128,1024]{1,0:T(8,128)S(1)} %fusion.37, bf16[128,2048]{1,0:T(8,128)(2,1)S(1)} %reshape.104, bf16[1,2048,1024]{2,1,0:T(8,128)(2,1)} %param.40), kind=kOutput, calls=%fused_computation.13 | convolution fusion | flops 1075183616 | bytes 9961472 | tf_op jit(solution)/shard_map/dot_general | solution.py:97
  169.3 4.2 %all_to_all.36 = bf16[2,128,1024]{2,1,0:T(8,128)(2,1)S(1)} all-to-all(bf16[2,128,1024]{2,1,0:T(8,128)(2,1)S(1)} %bitcast.69), channel_id=1, replica_groups=mesh['ep'=64,'tp'=2] {'tp'}, dimensions={0} | all-to-all | bytes 1048576 | tf_op jit(solution)/shard_map/all_to_all | solution.py:45
  173.5 0.8 convert_element_type.114
  174.4 74.0 %all-gather.5.cloned.1.call-done = bf16[2048,6144]{1,0:T(8,128)(2,1)} async-done(((bf16[32,6144]{1,0:T(8,128)(2,1)}), bf16[2048,6144]{1,0:T(8,128)(2,1)}) %all-gather.5.cloned.1.call-update) | async-done | bytes 25165840 | tf_op jit(solution)/shard_map/all_gather | solution.py:22
  248.4 5.6 %fusion.4 = f32[16,2048]{1,0:T(8,128)S(1)} fusion(bf16[16,2048]{1,0:T(8,128)(2,1)S(1)} %multiply_convert_fusion, bf16[2048,6144]{1,0:T(8,128)(2,1)} %all-gather.5.cloned.1.call-done), kind=kOutput, calls=%fused_computation.4 | convolution fusion | flops 134217728 | bytes 8585216 | tf_op jit(solution)/shard_map/td,fd->tf/dot_general | solution.py:196
  254.0 9.2 %fusion.21 = bf16[16,2048]{1,0:T(8,128)(2,1)S(1)} fusion(bf16[2048,6144]{1,0:T(8,128)(2,1)} %all-gather.5.cloned.1.call-done, bf16[16,2048]{1,0:T(8,128)(2,1)S(1)} %multiply_convert_fusion, f32[16,2048]{1,0:T(8,128)S(1)} %fusion.4), kind=kOutput, calls=%fused_computation.17 | convolution fusion | flops 268664832 | bytes 17039360 | tf_op jit(solution)/shard_map/dot_general | solution.py:201
  263.2 3.8 %all_to_all.37 = bf16[2,16,1024]{2,1,0:T(8,128)(2,1)S(1)} all-to-all(bf16[2,16,1024]{2,1,0:T(8,128)(2,1)S(1)} %bitcast.73), channel_id=1, replica_groups=mesh['ep'=64,'tp'=2] {'tp'}, dimensions={0} | all-to-all | bytes 131072 | tf_op jit(solution)/shard_map/all_to_all | solution.py:45
  267.0 8.6 %all-to-all-start.4 = ((bf16[64,2,1024]{2,1,0:T(2,128)(2,1)}), bf16[64,2,1024]{2,1,0:T(2,128)(2,1)S(1)}, u32[]{:S(2)}, u32[]{:S(2)}) async-start(bf16[64,2,1024]{2,1,0:T(2,128)(2,1)} %convert_element_type.114), calls=%async_computation.4 | async-start | bytes 524288 | tf_op jit(solution)/shard_map/all_to_all | solution.py:187
  275.8 10.8 %all-to-all-done.4 = bf16[64,2,1024]{2,1,0:T(2,128)(2,1)S(1)} async-done(((bf16[64,2,1024]{2,1,0:T(2,128)(2,1)}), bf16[64,2,1024]{2,1,0:T(2,128)(2,1)S(1)}, u32[]{:S(2)}, u32[]{:S(2)}) %all-to-all-start.4) | async-done | bytes 262176 | tf_op jit(solution)/shard_map/all_to_all | solution.py:187
  286.5 0.9 fusion.54
  (58 shorter events, 2.0 us)
Async XLA Ops:
  7.2 19.0 %copy-start.3 = (s32[16,4]{0,1:T(4,128)S(1)}, s32[16,4]{0,1:T(4,128)}, u32[]{:S(2)}) copy-start(s32[16,4]{0,1:T(4,128)} %param.37) | copy-start | bytes 772
  7.2 19.4 %copy-start.1 = (bf16[16,2048]{1,0:T(8,128)(2,1)S(1)}, bf16[16,2048]{1,0:T(8,128)(2,1)}, u32[]{:S(2)}) copy-start(bf16[16,2048]{1,0:T(8,128)(2,1)} %param.23) | copy-start | bytes 196612
  7.2 103.7 %copy-start.8 = (f32[2048]{0:T(1024)S(1)}, f32[2048]{0:T(1024)}, u32[]{:S(2)}) copy-start(f32[2048]{0:T(1024)} %param.24) | copy-start | bytes 24580
  7.2 103.6 %all-gather.3.cloned.1.call-start = ((), (), s32[]{:S(2)}) async-start(), calls=%async_computation.6 | async-start | bytes 9052160 | tf_op jit(solution)/shard_map/all_gather | solution.py:22
  10.4 101.8 %copy-start.9 = (f32[16,4]{0,1:T(4,128)S(1)}, f32[16,4]{0,1:T(4,128)}, u32[]{:S(2)}) copy-start(f32[16,4]{0,1:T(4,128)} %param.33) | copy-start | bytes 772
  10.4 101.8 %copy-start.10 = (f32[4]{0:T(128)S(1)}, f32[4]{0:T(128)}, u32[]{:S(2)}) copy-start(f32[4]{0:T(128)} %param.31) | copy-start | bytes 52
  10.4 238.0 %all-gather.5.cloned.1.call-start = ((), (), s32[]{:S(2)}) async-start(), calls=%async_computation.7 | async-start | bytes 25559040 | tf_op jit(solution)/shard_map/all_gather | solution.py:22
  14.6 114.3 %all-to-all-start = ((bf16[512,64,32]{0,2,1:T(8,128)(2,1)}), bf16[512,64,32]{0,2,1:T(8,128)(2,1)S(1)}, u32[]{:S(2)}, u32[]{:S(2)}) async-start(bf16[512,64,32]{0,2,1:T(8,128)(2,1)} %tile.2), calls=%async_computation | async-start | bytes 4194304 | tf_op jit(solution)/shard_map/all_to_all | solution.py:14
  113.8 8.3 %copy-start.5 = (f32[16,4]{0,1:T(4,128)}, f32[16,4]{0,1:T(4,128)S(1)}, u32[]{:S(2)}) copy-start(f32[16,4]{0,1:T(4,128)S(1)} %get-tuple-element.6) | copy-start | bytes 772
  125.5 2.0 copy-start
  127.5 1.3 copy-start.4
  127.5 6.1 %copy-start.2 = (f32[2048]{0:T(1024)S(1)}, f32[2048]{0:T(1024)}, u32[]{:S(2)}) copy-start(f32[2048]{0:T(1024)} %param.36) | copy-start | bytes 24580
  254.0 21.6 %copy-start.6 = (f32[2048]{0:T(1024)S(1)}, f32[2048]{0:T(1024)}, u32[]{:S(2)}) copy-start(f32[2048]{0:T(1024)} %param.45) | copy-start | bytes 24580
  254.0 21.6 %copy-start.7 = (f32[16,4]{0,1:T(4,128)S(1)}, f32[16,4]{0,1:T(4,128)}, u32[]{:S(2)}) copy-start(f32[16,4]{0,1:T(4,128)} %param.38) | copy-start | bytes 772
  267.0 19.5 %all-to-all-start.4 = ((bf16[64,2,1024]{2,1,0:T(2,128)(2,1)}), bf16[64,2,1024]{2,1,0:T(2,128)(2,1)S(1)}, u32[]{:S(2)}, u32[]{:S(2)}) async-start(bf16[64,2,1024]{2,1,0:T(2,128)(2,1)} %convert_element_type.114), calls=%async_computation.4 | async-start | bytes 524288 | tf_op jit(solution)/shard_map/all_to_all | solution.py:187
Sparse Core Ops, SparseCore 0:
  11.4 99.4 all-gather.2
  113.6 134.7 all-gather.4
